TPU v7x, 256 devices: a 4x2x16 block of a 4x16x16 slice. The times are simulated.
256 devices in a mesh: grp: 2 (over y), sp: 16 (over z), tp: 8 (over x, core).
Axes of the slice: x: 4, y: 2, z: 16, core: 2. Of those that a mesh axis runs over, the one named last changes fastest.
The devices are a block of a 4x16x16 slice.
Arguments:
- latent: bfloat16 [8192, 2048], P(('grp', 'sp', 'tp')), parts along dimension 0, may hold values from -6 to 6
- cond: bfloat16 [4096], P(('grp', 'sp')), parts along dimension 0, may hold values from -6 to 6
- context: bfloat16 [2048, 2048], P(('grp', 'sp')), parts along dimension 0, may hold values from -6 to 6
- context_cond: bfloat16 [2048], P('sp'), may hold values from -6 to 6
- norm_gain: bfloat16 [2048], replicated, may hold values from 0.099609375 to 1.8984375
- mod_shift: bfloat16 [2048, 2048], P('sp', 'tp'), may hold values from -0.125 to 0.125
- mod_scale: bfloat16 [2048, 2048], P('sp', 'tp'), may hold values from -0.125 to 0.125
- mod_gate: bfloat16 [2048, 2048], P('sp', 'tp'), may hold values from -0.125 to 0.125
- w_query: bfloat16 [2048, 2048], P(None, 'tp'), may hold values from -0.125 to 0.125
- w_key: bfloat16 [2048, 2048], P(None, 'tp'), may hold values from -0.125 to 0.125
- w_value: bfloat16 [2048, 4096], P(None, 'tp'), may hold values from -0.125 to 0.125
- w_gate: bfloat16 [2048, 4096], P(None, 'tp'), may hold values from -0.125 to 0.125
- w_out: bfloat16 [4096, 2048], P('tp'), may hold values from -0.09375 to 0.09375
- decay_rate: float32 [2, 8], P(None, 'tp'), may hold values from 3.90625e-05 to 0.034
- context_gain: float32 [8], P('tp'), may hold values from 3 to 10
Outputs:
- mixed: bfloat16 [8192, 2048], P(('grp', 'sp', 'tp')), parts along dimension 0
There are 2 independent parts, one for each index of `grp`. A program takes and returns all parts, laid end to end along the dimension named above; an argument that names none is the same for every part. Nothing has to cross between parts.
All inputs are finite; a program needn't handle non-finite values.
Results may differ from a plain program's by a relative error of at most 0.009.
Values may be sent and summed in bfloat16 or wider, within the bound.
A program may use at most 128 MiB of HBM per device.

v0:
```python
import jax
import jax.numpy as jnp
from jax import lax
from jax.sharding import PartitionSpec as P

DK = 256
GRID_W = 128
BLOCK = 128


norm_eps = 1e-06
rope_base = 10000.0


def copy_for_each(x, axis):
    copies = jnp.broadcast_to(x, (lax.axis_size(axis), *x.shape))
    return lax.all_to_all(copies, axis, split_axis=0, concat_axis=0, tiled=True)


def of_everyone(x, axis):
    return copy_for_each(x, axis).sum(axis=0)


def together(arrays, axis):
    ends = [0]
    for a in arrays:
        ends.append(ends[-1] + a.size)
    so_far = of_everyone(jnp.concatenate([a.ravel() for a in arrays]), axis)
    return tuple((so_far[b:e].reshape(a.shape) for a, b, e in zip(arrays, ends, ends[1:])))


def in_one_piece(arrays, axis, dim, along):
    widths = [a.shape[along] for a in arrays]
    both = jnp.concatenate(arrays, axis=along)
    whole = lax.all_gather(both, axis, axis=dim, tiled=True)
    return tuple(jnp.split(whole, [sum(widths[:k]) for k in range(1, len(widths))], axis=along))


def laid_out(blocks, dim):
    blocks = jnp.moveaxis(blocks, 0, dim)
    shape = blocks.shape
    return blocks.reshape(*shape[:dim], shape[dim] * shape[dim + 1], *shape[dim + 2 :])


def gather_directly(x, axis, dim):
    return laid_out(copy_for_each(x, axis), dim)


def prefix(x, axis, combine, identity, reverse):
    count, here = (lax.axis_size(axis), lax.axis_index(axis))
    everything = jax.tree.map(
        lambda part, kind: lax.all_gather(part.astype(kind), axis), x, (jnp.bfloat16, jnp.bfloat16)
    )
    start = jax.tree.map(
        lambda part, zero: jnp.broadcast_to(jnp.asarray(zero, part.dtype), part.shape), x, identity
    )

    def lap(k, before):
        at = count - 1 - k if reverse else k
        reached = at > here if reverse else at < here
        new = combine(
            before, jax.tree.map(lambda part, own: part[at].astype(own.dtype), everything, x)
        )
        return jax.tree.map(lambda a, b: jnp.where(reached, a, b), new, before)

    return lax.fori_loop(0, count, lap, start)


def in_blocks(x, dim, count):
    shape = x.shape
    blocks = x.reshape(*shape[:dim], count, shape[dim] // count, *shape[dim + 1 :])
    return jnp.moveaxis(blocks, dim, 0)


def sent_and_summed(x, axis, dim):
    count = lax.axis_size(axis)
    blocks = lax.all_to_all(in_blocks(x, dim, count), axis, 0, 0, tiled=True)
    return jnp.sum(blocks.astype(jnp.float32), axis=0)


def modulated(rows, norm_gain, shift, scale):
    values = rows.astype(jnp.float32)
    normed = values * lax.rsqrt(jnp.mean(values * values, axis=-1, keepdims=True) + norm_eps)
    return (normed * norm_gain.astype(jnp.float32) * (1.0 + scale) + shift).astype(jnp.bfloat16)


def rotate(vectors, positions):
    depth = vectors.shape[-1]
    freqs = depth // 4
    inv_freq = rope_base ** (-jnp.arange(freqs, dtype=jnp.float32) / freqs)
    grid_row = (positions // GRID_W).astype(jnp.float32)
    grid_col = (positions % GRID_W).astype(jnp.float32)
    angles = jnp.concatenate([grid_row[:, None] * inv_freq, grid_col[:, None] * inv_freq], axis=-1)[
        :, None, :
    ]
    cos_table = jnp.cos(angles)
    sin_table = jnp.sin(angles)
    first_half, second_half = jnp.split(vectors, 2, axis=-1)
    return jnp.concatenate(
        [
            first_half * cos_table - second_half * sin_table,
            second_half * cos_table + first_half * sin_table,
        ],
        axis=-1,
    )


def context_states(ctx_key, ctx_value, fwd_rate, bwd_rate, context_gain):
    total = ctx_key.shape[0]
    place = jnp.arange(total, dtype=jnp.float32)[:, None]
    fwd_weight = jnp.exp(-fwd_rate[None, :] * (total - 1.0 - place))
    bwd_weight = jnp.exp(-bwd_rate[None, :] * place)
    fwd_keys = (ctx_key.astype(jnp.float32) * fwd_weight[:, :, None]).astype(jnp.bfloat16)
    bwd_keys = (ctx_key.astype(jnp.float32) * bwd_weight[:, :, None]).astype(jnp.bfloat16)
    fwd_state = jnp.einsum("jhd,jhe->hde", fwd_keys, ctx_value, preferred_element_type=jnp.float32)
    bwd_state = jnp.einsum("jhd,jhe->hde", bwd_keys, ctx_value, preferred_element_type=jnp.float32)
    return (fwd_state * context_gain[:, None, None], bwd_state * context_gain[:, None, None])


def join_carry(earlier, later):
    return (earlier[0] * later[1][:, None, None] + later[0], earlier[1] * later[1])


def body(
    latent,
    cond,
    context,
    context_cond,
    norm_gain,
    mod_shift,
    mod_scale,
    mod_gate,
    w_query,
    w_key,
    w_value,
    w_gate,
    w_out,
    decay_rate,
    context_gain,
):
    head_count = w_query.shape[1] // DK
    value_width = w_value.shape[1] // head_count
    local_rows = latent.shape[0]
    span = local_rows * lax.axis_size("tp")
    seq_index = lax.axis_index("sp")
    cond_rows = jax.nn.silu(jnp.stack([cond, context_cond]).astype(jnp.float32)).astype(
        jnp.bfloat16
    )
    shift_part = jnp.dot(cond_rows, mod_shift, preferred_element_type=jnp.float32)
    scale_part = jnp.dot(cond_rows, mod_scale, preferred_element_type=jnp.float32)
    gate_part = jnp.dot(cond_rows[0:1], mod_gate, preferred_element_type=jnp.float32)
    shift_sum, scale_sum, gate_sum = together((shift_part, scale_part, gate_part), "sp")
    shift, scale, gate = in_one_piece((shift_sum, scale_sum, gate_sum), "tp", 1, 0)
    h_latent = modulated(latent, norm_gain, shift[0], scale[0])
    piece = gather_directly(h_latent, "tp", 0)
    projected = jnp.concatenate(
        [
            jnp.dot(piece, weight, preferred_element_type=jnp.float32)
            for weight in (w_query, w_key, w_value, w_gate)
        ],
        axis=1,
    )
    key_cols = head_count * DK
    val_cols = head_count * value_width
    positions = seq_index * span + jnp.arange(span, dtype=jnp.int32)
    query = rotate(projected[:, :key_cols].reshape(span, head_count, DK), positions).astype(
        jnp.bfloat16
    )
    keys = rotate(
        projected[:, key_cols : 2 * key_cols].reshape(span, head_count, DK) * DK ** (-0.5),
        positions,
    ).astype(jnp.bfloat16)
    values = (
        projected[:, 2 * key_cols : 2 * key_cols + val_cols]
        .astype(jnp.bfloat16)
        .reshape(span, head_count, value_width)
    )
    gate_pre = projected[:, 2 * key_cols + val_cols :].reshape(span, head_count, value_width)
    whole_context = lax.all_gather(context, "sp", axis=0, tiled=True)
    h_context = modulated(whole_context, norm_gain, shift[1], scale[1])
    ctx_key = (jnp.dot(h_context, w_key, preferred_element_type=jnp.float32) * DK ** (-0.5)).astype(
        jnp.bfloat16
    )
    ctx_value = jnp.dot(h_context, w_value, preferred_element_type=jnp.float32).astype(jnp.bfloat16)
    ctx_total = ctx_key.shape[0]
    fwd_rate = decay_rate[0]
    bwd_rate = decay_rate[1]
    ctx_fwd, ctx_bwd = context_states(
        ctx_key.reshape(ctx_total, head_count, DK),
        ctx_value.reshape(ctx_total, head_count, value_width),
        fwd_rate,
        bwd_rate,
        context_gain,
    )
    blocks = span // BLOCK
    query_b = query.reshape(blocks, BLOCK, head_count, DK)
    keys_b = keys.reshape(blocks, BLOCK, head_count, DK)
    values_b = values.reshape(blocks, BLOCK, head_count, value_width)
    place = jnp.arange(BLOCK, dtype=jnp.float32)
    gap = place[:, None] - place[None, :]
    mask = jnp.where(
        gap >= 0, jnp.exp(-fwd_rate[:, None, None] * jnp.maximum(gap, 0.0)), 0.0
    ) + jnp.where(gap <= 0, jnp.exp(-bwd_rate[:, None, None] * jnp.maximum(-gap, 0.0)), 0.0)
    scores = jnp.einsum("bihd,bjhd->bhij", query_b, keys_b, preferred_element_type=jnp.float32)
    weights = (scores * mask[None]).astype(jnp.bfloat16)
    retained = jnp.einsum("bhij,bjhe->bihe", weights, values_b, preferred_element_type=jnp.float32)
    fwd_kw = jnp.exp(-fwd_rate[None, :] * (BLOCK - 1.0 - place[:, None]))
    bwd_kw = jnp.exp(-bwd_rate[None, :] * place[:, None])
    fwd_keys = (keys_b.astype(jnp.float32) * fwd_kw[None, :, :, None]).astype(jnp.bfloat16)
    bwd_keys = (keys_b.astype(jnp.float32) * bwd_kw[None, :, :, None]).astype(jnp.bfloat16)
    fwd_blocks = jnp.einsum(
        "bjhd,bjhe->bhde", fwd_keys, values_b, preferred_element_type=jnp.float32
    )
    bwd_blocks = jnp.einsum(
        "bjhd,bjhe->bhde", bwd_keys, values_b, preferred_element_type=jnp.float32
    )
    order = jnp.arange(blocks, dtype=jnp.float32)
    fwd_local = jnp.einsum(
        "bh,bhde->hde",
        jnp.exp(-fwd_rate[None, :] * BLOCK * (blocks - 1.0 - order[:, None])),
        fwd_blocks,
    )
    bwd_local = jnp.einsum(
        "bh,bhde->hde", jnp.exp(-bwd_rate[None, :] * BLOCK * order[:, None]), bwd_blocks
    )
    unit = jnp.ones((head_count,), jnp.float32)
    blank = jnp.zeros_like(fwd_local)
    fwd_in, fwd_decay = prefix(
        (fwd_local, jnp.exp(-fwd_rate * span)), "sp", join_carry, (blank, unit), False
    )
    bwd_in, bwd_decay = prefix(
        (bwd_local, jnp.exp(-bwd_rate * span)), "sp", join_carry, (blank, unit), True
    )
    fwd_start = fwd_in + fwd_decay[:, None, None] * ctx_fwd
    bwd_start = bwd_in + bwd_decay[:, None, None] * ctx_bwd
    lag = order[:, None] - order[None, :]
    fwd_mix = jnp.where(
        lag[:, :, None] > 0,
        jnp.exp(-fwd_rate[None, None, :] * BLOCK * jnp.maximum(lag - 1.0, 0.0)[:, :, None]),
        0.0,
    )
    bwd_mix = jnp.where(
        lag[:, :, None] < 0,
        jnp.exp(-bwd_rate[None, None, :] * BLOCK * jnp.maximum(-lag - 1.0, 0.0)[:, :, None]),
        0.0,
    )
    fwd_enter = (
        jnp.einsum("cbh,bhde->chde", fwd_mix, fwd_blocks)
        + jnp.exp(-fwd_rate[None, :] * BLOCK * order[:, None])[:, :, None, None] * fwd_start[None]
    )
    bwd_enter = (
        jnp.einsum("cbh,bhde->chde", bwd_mix, bwd_blocks)
        + jnp.exp(-bwd_rate[None, :] * BLOCK * (blocks - 1.0 - order[:, None]))[:, :, None, None]
        * bwd_start[None]
    )
    fwd_qw = jnp.exp(-fwd_rate[None, :] * (place[:, None] + 1.0))[None, :, :, None]
    bwd_qw = jnp.exp(-bwd_rate[None, :] * (BLOCK - place[:, None]))[None, :, :, None]
    fwd_cross = jnp.einsum(
        "bihd,bhde->bihe",
        query_b,
        fwd_enter.astype(jnp.bfloat16),
        preferred_element_type=jnp.float32,
    )
    bwd_cross = jnp.einsum(
        "bihd,bhde->bihe",
        query_b,
        bwd_enter.astype(jnp.bfloat16),
        preferred_element_type=jnp.float32,
    )
    retained = retained + fwd_cross * fwd_qw + bwd_cross * bwd_qw
    retained = retained.reshape(span, head_count, value_width)
    centre = jnp.mean(retained, axis=-1, keepdims=True)
    variance = jnp.mean(jnp.square(retained - centre), axis=-1, keepdims=True)
    normed = (retained - centre) * lax.rsqrt(variance + norm_eps)
    gated = (
        (jax.nn.silu(gate_pre) * normed)
        .astype(jnp.bfloat16)
        .reshape(span, head_count * value_width)
    )
    output_sum = sent_and_summed(
        jnp.dot(gated, w_out, preferred_element_type=jnp.float32).astype(jnp.bfloat16), "tp", 0
    )
    return (latent.astype(jnp.float32) + gate[0] * output_sum).astype(jnp.bfloat16)


def solution(mesh):
    return jax.shard_map(
        body,
        mesh=mesh,
        in_specs=(
            P(("grp", "sp", "tp"), None),
            P(("grp", "sp")),
            P(("grp", "sp"), None),
            P("sp"),
            P(),
            P("sp", "tp"),
            P("sp", "tp"),
            P("sp", "tp"),
            P(None, "tp"),
            P(None, "tp"),
            P(None, "tp"),
            P(None, "tp"),
            P("tp", None),
            P(None, "tp"),
            P("tp"),
        ),
        out_specs=P(("grp", "sp", "tp"), None),
        check_vma=False,
    )
```

profile of v0, /device:TPU:33, one launch (start us, length us, event | category | flops | bytes accessed | tf_op | source)
XLA Modules:
  0.0 337.2 jit_solution(15199931979593779652)
XLA Ops:
  11.6 24.5 %all-to-all-start = ((f32[16,1,1280]{2,1,0:T(1,128)}), f32[16,1,1280]{2,1,0:T(1,128)S(1)}, u32[]{:S(2)}, u32[]{:S(2)}) async-start(f32[16,1,1280]{2,1,0:T(1,128)} %broadcast_in_dim.16), calls=%async_computation | async-start | bytes 163840 | tf_op jit(solution)/shard_map/all_to_all | solution.py:17
  37.9 10.1 %all-to-all-done = f32[16,1,1280]{2,1,0:T(1,128)S(1)} async-done(((f32[16,1,1280]{2,1,0:T(1,128)}), f32[16,1,1280]{2,1,0:T(1,128)S(1)}, u32[]{:S(2)}, u32[]{:S(2)}) %all-to-all-start) | async-done | bytes 81952 | tf_op jit(solution)/shard_map/all_to_all | solution.py:17
  48.1 15.8 %all_gather.26 = f32[5,2048]{1,0:T(8,128)S(1)} all-gather(f32[5,256]{1,0:T(8,128)S(1)} %pad_maximum_fusion.12), channel_id=1, replica_groups=mesh['grp'=2,'sp'=16,'tp'=8] {'tp'}, dimensions={1}, use_global_device_ids=true | all-gather | bytes 46080 | tf_op jit(solution)/shard_map/all_gather | solution.py:35
  66.7 4.2 %all-to-all-start.1 = ((bf16[8,32,2048]{2,1,0:T(8,128)(2,1)}), bf16[8,32,2048]{2,1,0:T(8,128)(2,1)S(1)}, u32[]{:S(2)}, u32[]{:S(2)}) async-start(bf16[8,32,2048]{2,1,0:T(8,128)(2,1)} %broadcast_in_dim.17), calls=%async_computation.1 | async-start | bytes 2097152 | tf_op jit(solution)/shard_map/all_to_all | solution.py:17
  73.5 12.3 %all-to-all-done.1 = bf16[8,32,2048]{2,1,0:T(8,128)(2,1)S(1)} async-done(((bf16[8,32,2048]{2,1,0:T(8,128)(2,1)}), bf16[8,32,2048]{2,1,0:T(8,128)(2,1)S(1)}, u32[]{:S(2)}, u32[]{:S(2)}) %all-to-all-start.1) | async-done | bytes 1048608 | tf_op jit(solution)/shard_map/all_to_all | solution.py:17
  85.8 2.1 convolution_bitcast_fusion.5
  98.7 23.5 %all-reduce.2 = (bf16[16]{0:T(256)(128)(2,1)}, bf16[16]{0:T(256)(128)(2,1)}) all-reduce(bf16[16]{0:T(256)(128)(2,1)S(1)} %dynamic-update-slice.1, bf16[16]{0:T(256)(128)(2,1)S(1)} %dynamic-update-slice), channel_id=1, replica_groups=mesh['grp'=2,'sp'=16,'tp'=8] {'sp'}, use_global_device_ids=true, to_apply=%add.1 | all-reduce | flops 32 | bytes 128
  126.5 2.1 convolution_bitcast_fusion.4
  128.6 3.3 fusion.2
  132.1 3.8 %fusion.7 = bf16[1024,256]{1,0:T(8,128)(2,1)} fusion(bf16[2048,256]{1,0:T(8,128)(2,1)} %param.28, bf16[1024,2048]{1,0:T(8,128)(2,1)S(1)} %copy-done.3, f32[2048]{0:T(1024)S(1)} %bitcast.219, f32[2048]{0:T(1024)S(1)} %bitcast.221, f32[2048]{0:T(1024)S(1)} %convert_element_type.203, f32[1024]{0:T(1024)S(1)} %add_rsqrt_fusion), kind=kOutput, calls=%fused_computation.21 | convolution fusion | flops 1086849024 | bytes 5795840 | tf_op jit(solution)/shard_map/dot_general | solution.py:181
  135.9 3.4 %convolution_convert_fusion.1 = bf16[1024,512]{1,0:T(8,128)(2,1)} fusion(bf16[2048,512]{1,0:T(8,128)(2,1)S(1)} %copy-done, bf16[1024,2048]{1,0:T(8,128)(2,1)S(1)} %copy-done.3, f32[2048]{0:T(1024)S(1)} %bitcast.220, f32[2048]{0:T(1024)S(1)} %bitcast.222, f32[2048]{0:T(1024)S(1)} %convert_element_type.203, f32[1024]{0:T(1024)S(1)} %add_rsqrt_fusion), kind=kOutput, calls=%fused_computation.15 | convolution fusion | flops 2160590848 | bytes 7368704 | tf_op jit(solution)/shard_map/dot_general | solution.py:184
  139.3 27.3 %all-gather.10.cloned.1.call-done = bf16[4096,512]{1,0:T(8,128)(2,1)} async-done(((bf16[256,512]{1,0:T(8,128)(2,1)}), bf16[4096,512]{1,0:T(8,128)(2,1)}) %all-gather.10.cloned.1.call-update) | async-done | bytes 4194320 | tf_op jit(solution)/shard_map/all_gather | solution.py:52
  166.7 50.8 %while.35 = (s32[]{:T(128)}, f32[1,256,512]{2,1,0:T(8,128)S(1)}, f32[1]{0:T(128)}, s32[]{:T(128)}, bf16[16,1]{0,1:T(2,128)(2,1)S(1)}, /*index=5*/bf16[16,1,256,5...) while((s32[]{:T(128)}, f32[1,256,512]{2,1,0:T(8,128)S(1)}, f32[1]{0:T(128)}, ...), condition=%wide.region_6.7_spmd.clone, body=%wide.region_5.6_spmd.clone.sunk | while | flops 655371 | bytes 1310938 | solution.py:66
  167.3 1.9 fusion.150
  170.4 1.9 fusion.150
  173.6 1.9 fusion.150
  176.8 1.9 fusion.150
  180.0 1.9 fusion.150
  183.1 1.9 fusion.150
  186.3 1.9 fusion.150
  189.5 1.9 fusion.150
  192.7 1.9 fusion.150
  195.9 1.9 fusion.150
  199.0 1.9 fusion.150
  202.2 1.9 fusion.150
  205.4 1.9 fusion.150
  208.6 1.9 fusion.150
  211.8 1.9 fusion.150
  214.9 1.9 fusion.150
  217.5 24.4 %all-gather.8.cloned.1.call-done = bf16[4096,512]{1,0:T(8,128)(2,1)} async-done(((bf16[256,512]{1,0:T(8,128)(2,1)}), bf16[4096,512]{1,0:T(8,128)(2,1)}) %all-gather.8.cloned.1.call-update) | async-done | bytes 4194320 | tf_op jit(solution)/shard_map/all_gather | solution.py:52
  241.9 50.7 %while.34 = (s32[]{:T(128)}, f32[1,256,512]{2,1,0:T(8,128)S(1)}, f32[1]{0:T(128)}, s32[]{:T(128)}, bf16[16,1]{0,1:T(2,128)(2,1)S(1)}, /*index=5*/bf16[16,1,256,512]{3,2,1,0:T(8,128)(2,1)}, s32[]{:T(128)}, s32[]{:T(128)}) while((s32[]{:T(128)}, f32[1,256,512]{2,1,0:T(8,128)S(1)}, f32[1]{0:T(128)}, s32[]{:T(128)}, ...), condition=%wide.region_3.4_spmd.clone, body=%wide.region_2.3_spmd.clone.sunk | while | flops 655367 | bytes 1310876 | solution.py:66
  242.5 1.9 fusion.148
  245.7 1.9 fusion.148
  248.8 1.9 fusion.148
  252.0 1.9 fusion.148
  255.2 1.9 fusion.148
  258.4 1.9 fusion.148
  261.5 1.9 fusion.148
  264.7 1.9 fusion.148
  267.9 1.9 fusion.148
  271.0 1.9 fusion.148
  274.2 1.9 fusion.148
  277.4 1.9 fusion.148
  280.5 1.9 fusion.148
  290.0 1.9 fusion.148
  292.7 2.3 fusion.23
  295.0 2.0 fusion.16
  301.4 28.4 %all_to_all.16 = bf16[8,32,2048]{2,1,0:T(8,128)(2,1)S(1)} all-to-all(bf16[8,32,2048]{2,1,0:T(8,128)(2,1)S(1)} %bitcast.196), channel_id=1, replica_groups=mesh['grp'=2,'sp'=16,'tp'=8] {'tp'}, dimensions={0} | all-to-all | bytes 2097152 | tf_op jit(solution)/shard_map/all_to_all | solution.py:77
  (162 shorter events, 53.1 us)
Async XLA Ops:
  6.5 83.7 %copy-start = (bf16[2048,512]{1,0:T(8,128)(2,1)S(1)}, bf16[2048,512]{1,0:T(8,128)(2,1)}, u32[]{:S(2)}) copy-start(bf16[2048,512]{1,0:T(8,128)(2,1)} %param.29) | copy-start | bytes 6291460
  6.6 64.3 %copy-start.20 = (f32[2,1]{0,1:T(1,128)S(1)}, f32[2,1]{0,1:T(1,128)}, u32[]{:S(2)}) copy-start(f32[2,1]{0,1:T(1,128)} %param.32) | copy-start | bytes 28
  6.6 122.0 %all-gather.6.cloned.1.call-start = ((), (), s32[]{:S(2)}) async-start(), calls=%async_computation.3 | async-start | bytes 4456448 | tf_op jit(solution)/shard_map/all_gather | solution.py:179
  11.6 36.3 %all-to-all-start = ((f32[16,1,1280]{2,1,0:T(1,128)}), f32[16,1,1280]{2,1,0:T(1,128)S(1)}, u32[]{:S(2)}, u32[]{:S(2)}) async-start(f32[16,1,1280]{2,1,0:T(1,128)} %broadcast_in_dim.16), calls=%async_computation | async-start | bytes 163840 | tf_op jit(solution)/shard_map/all_to_all | solution.py:17
  66.7 19.1 %all-to-all-start.1 = ((bf16[8,32,2048]{2,1,0:T(8,128)(2,1)}), bf16[8,32,2048]{2,1,0:T(8,128)(2,1)S(1)}, u32[]{:S(2)}, u32[]{:S(2)}) async-start(bf16[8,32,2048]{2,1,0:T(8,128)(2,1)} %broadcast_in_dim.17), calls=%async_computation.1 | async-start | bytes 2097152 | tf_op jit(solution)/shard_map/all_to_all | solution.py:17
  70.8 95.9 %all-gather.10.cloned.1.call-start = ((), (), s32[]{:S(2)}) async-start(), calls=%async_computation.5 | async-start | bytes 4456448 | tf_op jit(solution)/shard_map/all_gather | solution.py:52
  85.8 5.2 %copy-start.1 = (bf16[8,32,2048]{2,1,0:T(8,128)(2,1)}, bf16[8,32,2048]{2,1,0:T(8,128)(2,1)S(1)}, u32[]{:S(2)}) copy-start(bf16[8,32,2048]{2,1,0:T(8,128)(2,1)S(1)} %all-to-all-done.1) | copy-start | bytes 3145732
  85.8 3.8 %copy-start.14 = (f32[256,1,64]{2,0,1:T(8,128)S(1)}, f32[256,1,64]{2,0,1:T(8,128)}, u32[]{:S(2)}) copy-start(f32[256,1,64]{2,0,1:T(8,128)} %get-tuple-element.359) | copy-start | bytes 196612
  85.8 3.8 %copy-start.15 = (f32[256,1,64]{2,0,1:T(8,128)S(1)}, f32[256,1,64]{2,0,1:T(8,128)}, u32[]{:S(2)}) copy-start(f32[256,1,64]{2,0,1:T(8,128)} %get-tuple-element.360) | copy-start | bytes 196612
  87.9 3.1 copy-start.23
  90.2 0.7 copy-start.9
  90.2 1.2 copy-start.10
  91.4 1.5 copy-start.11
  91.4 5.1 %copy-start.25 = (u32[256]{0:T(256)S(1)}, u32[256]{0:T(256)}, u32[]{:S(2)}) copy-start(u32[256]{0:T(256)} %constant.167) | copy-start | bytes 3076
  92.9 149.0 %all-gather.8.cloned.1.call-start = ((), (), s32[]{:S(2)}) async-start(), calls=%async_computation.4 | async-start | bytes 4456448 | tf_op jit(solution)/shard_map/all_gather | solution.py:52
  94.9 1.5 copy-start.12
  128.6 3.3 copy-start.18
  128.6 3.3 copy-start.19
  128.6 3.5 %copy-start.3 = (bf16[1024,2048]{1,0:T(8,128)(2,1)S(1)}, bf16[1024,2048]{1,0:T(8,128)(2,1)}, u32[]{:S(2)}) copy-start(bf16[1024,2048]{1,0:T(8,128)(2,1)} %all-gather.6.cloned.1.call-done) | copy-start | bytes 12582916
  135.9 30.8 %copy-start.27 = (bf16[16]{0:T(256)(128)(2,1)S(1)}, bf16[16]{0:T(256)(128)(2,1)}, u32[]{:S(2)}) copy-start(bf16[16]{0:T(256)(128)(2,1)} %get-tuple-element.340) | copy-start | bytes 100
  139.3 102.6 %copy-start.26 = (bf16[16]{0:T(256)(128)(2,1)S(1)}, bf16[16]{0:T(256)(128)(2,1)}, u32[]{:S(2)}) copy-start(bf16[16]{0:T(256)(128)(2,1)} %get-tuple-element.341) | copy-start | bytes 100
  217.5 75.1 %copy-start.17 = (f32[1024]{0:T(1024)S(1)}, f32[1024]{0:T(1024)}, u32[]{:S(2)}) copy-start(f32[1024]{0:T(1024)} %multiply_exponential_fusion) | copy-start | bytes 12292
  241.9 53.0 %copy-start.29 = (f32[2]{0:T(128)S(1)}, f32[2]{0:T(128)}, u32[]{:S(2)}) copy-start(f32[2]{0:T(128)} %multiply_exponential_fusion.3) | copy-start | bytes 28
  292.6 4.4 %copy-start.21 = (f32[128]{0:T(128)S(1)}, f32[128]{0:T(128)}, u32[]{:S(2)}) copy-start(f32[128]{0:T(128)} %get-tuple-element.363) | copy-start | bytes 1540
  292.6 4.6 %copy-start.4 = (bf16[1024,512]{1,0:T(8,128)(2,1)S(1)}, bf16[1024,512]{1,0:T(8,128)(2,1)}, u32[]{:S(2)}) copy-start(bf16[1024,512]{1,0:T(8,128)(2,1)} %convolution_convert_fusion.1) | copy-start | bytes 3145732
  292.6 4.6 %copy-start.5 = (bf16[1024,256]{1,0:T(8,128)(2,1)S(1)}, bf16[1024,256]{1,0:T(8,128)(2,1)}, u32[]{:S(2)}) copy-start(bf16[1024,256]{1,0:T(8,128)(2,1)} %fusion.7) | copy-start | bytes 1572868
  292.7 4.6 %copy-start.16 = (f32[1024]{0:T(1024)S(1)}, f32[1024]{0:T(1024)}, u32[]{:S(2)}) copy-start(f32[1024]{0:T(1024)} %multiply_exponential_fusion.1) | copy-start | bytes 12292
  295.0 3.1 copy-start.13
  295.0 3.1 copy-start.28
  297.0 2.0 copy-start.6
  297.0 2.0 copy-start.22
  297.3 2.3 copy-start.2
  297.3 2.3 copy-start.24
  299.0 1.6 copy-start.7
  300.6 29.3 %copy-start.8 = (bf16[32,2048]{1,0:T(8,128)(2,1)S(1)}, bf16[32,2048]{1,0:T(8,128)(2,1)}, u32[]{:S(2)}) copy-start(bf16[32,2048]{1,0:T(8,128)(2,1)} %param.19) | copy-start | bytes 393220
Sparse Core Ops, SparseCore 0:
  9.2 83.4 all-gather.5
  94.4 72.1 all-gather.9
  168.5 73.3 all-gather.7
where the time goes:
time: 340 us; the launch traced here: 337 us
  other arithmetic  94.1 us (28%)
  waiting for transfers between devices  74.9 us (22%)
  blocking collectives  67.7 us (20%)
  starting transfers between devices  28.7 us (8%)
  matrix products  27.7 us (8%)
  loops' own time  21.6 us (6%)
  between operations  15.7 us (5%)
  local copies, waits for them, and re-layouts  6.64 us (2%)
    select_n x32, other arithmetic, lap(): return jax.tree.map(lambda a, b: jnp.where(reached, a, b), new, before)  61.2 us
    all_gather x2, waiting for transfers between devices, prefix(): lax.all_gather(part.astype(kind), axis)  51.7 us
    all_to_all x2, starting transfers between devices, copy_for_each(): return lax.all_to_all(copies, axis, split_axis=0, concat_axis=0, tiled=True)  28.7 us
    all_to_all x1, blocking collectives, sent_and_summed(): blocks = lax.all_to_all(in_blocks(x, dim, count), axis, 0, 0, tiled=True)  28.4 us
    unnamed x1, blocking collectives  23.5 us
    all_to_all x2, waiting for transfers between devices, copy_for_each(): return lax.all_to_all(copies, axis, split_axis=0, concat_axis=0, tiled=True)  22.4 us
    another operation x2, loops' own time, prefix(): return lax.fori_loop(0, count, lap, start)  21.6 us
    convert_element_type x32, other arithmetic, lap(): part[at].astype(own.dtype)  18.7 us
  transfers between devices with their start and end apart: 5, of which 4 were waited for; matrix products, arithmetic and copies ran while one was open for 23% of the time, Pallas kernels for 0%

commit v1 on v0

v1 whole, which is shorter than its diff:
```python
import functools

import jax
import jax.numpy as jnp
import numpy as np
from jax import lax
from jax.experimental import pallas as pl
from jax.experimental.pallas import tpu as pltpu
from jax.sharding import PartitionSpec as P

GRID_W = 128
norm_eps = 1e-06
rope_base = 10000.0
MESH = pl.DeviceIdType.MESH
F32 = jnp.float32
BF16 = jnp.bfloat16
LANES = 128
CHUNK = 8
LEAD = 6


def rope_tables(rows, freqs):
    inv_freq = (rope_base ** (-np.arange(freqs, dtype=np.float32) / np.float32(freqs))).astype(np.float32)
    row_angles = np.arange(rows, dtype=np.float32)[:, None] * inv_freq
    col_angles = np.arange(GRID_W, dtype=np.float32)[:, None] * inv_freq
    row_angles = np.concatenate([row_angles, row_angles], axis=1).astype(np.float64)
    col_angles = np.concatenate([col_angles, col_angles], axis=1).astype(np.float64)
    return np.concatenate(
        [np.cos(row_angles), np.cos(col_angles), np.sin(row_angles), np.sin(col_angles)]
    ).astype(np.float32)


def silu(v):
    return v / (1.0 + jnp.exp(-v))


def dot(a, b):
    return jnp.dot(a, b, preferred_element_type=F32)


def dot_tokens(a, b):
    return lax.dot_general(a, b, (((0,), (0,)), ((), ())), preferred_element_type=F32)


def kernel(
    n_sp,
    n_tp,
    decay_ref,
    cgain_ref,
    latent_hbm,
    cond_hbm,
    context_hbm,
    gain_hbm,
    shift_hbm,
    scale_hbm,
    gate_hbm,
    wq_hbm,
    wk_hbm,
    wv_hbm,
    wg_hbm,
    wo_hbm,
    tab_hbm,
    out_ref,
    x_ref,
    c_ref,
    cond_ref,
    gain_ref,
    mshift_ref,
    mscale_ref,
    mgate_ref,
    wq_ref,
    wk_ref,
    wv_ref,
    wg_ref,
    wo_ref,
    tab_ref,
    part_ref,
    gpart_ref,
    precv_ref,
    grecv_ref,
    modf_ref,
    gatef_ref,
    r_ref,
    h_ref,
    k_ref,
    v_ref,
    lf_ref,
    lb_ref,
    cf_ref,
    cb_ref,
    ps_ref,
    pr_ref,
    ms_ref,
    mr_ref,
    q_ref,
    gp_ref,
    ret_ref,
    g_ref,
    osend_ref,
    orecv_ref,
    own_ref,
    xsend_ref,
    xrecv_ref,
    load_sem,
    msend_sem,
    mrecv_sem,
    gsend_sem,
    grecv_sem,
    tsend_sem,
    trecv_sem,
    hsend_sem,
    hrecv_sem,
    xsend_sem,
    xrecv_sem,
    pssem,
    prsem,
    mssem,
    mrsem,
    osend_sem,
    orecv_sem,
    rsend_sem,
    rrecv_sem,
):
    s = lax.axis_index("sp")
    t = lax.axis_index("tp")
    n_x = n_tp // 2
    x = t // 2
    c = t % 2
    partner = x * 2 + (1 - c)
    rows = x_ref.shape[1]
    D = x_ref.shape[2]
    span = rows * n_tp
    ctx_rows = c_ref.shape[0]
    dk = wk_ref.shape[1]
    dv = wv_ref.shape[1]
    n_chunks = dk // CHUNK

    def load(k, src, dst):
        copy = pltpu.make_async_copy(src, dst, load_sem.at[k])
        copy.start()
        return copy

    l_lat = load(0, latent_hbm, x_ref.at[t])
    l_cond = load(1, cond_hbm, cond_ref)
    l_ms = load(2, shift_hbm, mshift_ref)
    l_mc = load(3, scale_hbm, mscale_ref)
    l_mg = load(4, gate_hbm, mgate_ref)
    l_ctx = load(5, context_hbm, c_ref)
    l_gain = load(6, gain_hbm, gain_ref)
    l_tab = load(7, tab_hbm, tab_ref)
    l_wk = load(8, wk_hbm, wk_ref)
    l_wv = load(9, wv_hbm, wv_ref)
    l_wq = load(10, wq_hbm, wq_ref)
    l_wg = load(11, wg_hbm, wg_ref)
    l_wo = load(12, wo_hbm, wo_ref)

    barrier = pltpu.get_barrier_semaphore()
    for d in range(n_sp // 2, 0, -1):
        pl.semaphore_signal(barrier, inc=1, device_id={"sp": (s + d) % n_sp}, device_id_type=MESH)
        if 2 * d != n_sp:
            pl.semaphore_signal(barrier, inc=1, device_id={"sp": (s + n_sp - d) % n_sp}, device_id_type=MESH)
    for d in range(1, n_tp):
        pl.semaphore_signal(barrier, inc=1, device_id={"tp": (t + d) % n_tp}, device_id_type=MESH)

    l_cond.wait()
    crows = silu(cond_ref[...].astype(F32))
    rid = lax.broadcasted_iota(jnp.int32, (8, crows.shape[1]), 0)
    cl = jnp.broadcast_to(crows[0:1], rid.shape)
    cc = jnp.broadcast_to(crows[1:2], rid.shape)
    lhs_shift = jnp.where(rid == 0, cl, jnp.where(rid == 1, cc, 0.0)).astype(BF16)
    lhs_scale = jnp.where(rid == 2, cl, jnp.where(rid == 3, cc, 0.0)).astype(BF16)
    lhs_gate = jnp.where(rid == 0, cl, 0.0).astype(BF16)
    l_ms.wait()
    l_mc.wait()
    part = dot(lhs_shift, mshift_ref[...]) + dot(lhs_scale, mscale_ref[...])
    part_ref[...] = part[0:4]
    l_mg.wait()
    gpart_ref[...] = dot(lhs_gate, mgate_ref[...])[0:1]
    l_lat.wait()

    pl.semaphore_wait(barrier, n_sp - 1 + n_tp - 1)

    def sp_copy(d):
        return pltpu.make_async_remote_copy(
            src_ref=part_ref,
            dst_ref=precv_ref.at[d - 1],
            send_sem=msend_sem.at[d - 1],
            recv_sem=mrecv_sem.at[d - 1],
            device_id={"sp": (s + d) % n_sp},
            device_id_type=MESH,
        )

    def spg_copy(d):
        return pltpu.make_async_remote_copy(
            src_ref=gpart_ref,
            dst_ref=grecv_ref.at[d - 1],
            send_sem=gsend_sem.at[d - 1],
            recv_sem=grecv_sem.at[d - 1],
            device_id={"sp": (s + d) % n_sp},
            device_id_type=MESH,
        )

    order = [n_sp // 2]
    for d in range(n_sp // 2 - 1, 0, -1):
        order += [d, n_sp - d]
    for d in order:
        sp_copy(d).start()

    def lat_copy(block, to, sem):
        return pltpu.make_async_remote_copy(
            src_ref=x_ref.at[block],
            dst_ref=x_ref.at[block],
            send_sem=xsend_sem.at[sem],
            recv_sem=xrecv_sem.at[block],
            device_id={"tp": to},
            device_id_type=MESH,
        )

    hops = [1, n_x - 1] + list(range(2, n_x - 1))
    for d in hops:
        lat_copy(t, ((x + d) % n_x) * 2 + c, d).start()
    lat_copy(t, partner, 0).start()
    for d in order:
        spg_copy(d).start()

    l_ctx.wait()
    cv = c_ref[...].astype(F32)
    r = lax.rsqrt(jnp.mean(cv * cv, axis=-1, keepdims=True) + norm_eps)
    r_ref[pl.ds(span, ctx_rows), :] = jnp.broadcast_to(r, (ctx_rows, LANES))

    def forward(d):
        block = ((x + d) % n_x) * 2 + c
        lat_copy(block, block, d).wait_recv()
        lat_copy(block, partner, n_x + d).start()

    for d in hops[:2]:
        forward(d)

    total = part_ref[...]
    for d in range(1, n_sp):
        sp_copy(d).wait_recv()
        total = total + precv_ref[d - 1]
    modf_ref[t] = total

    def tp_copy(d, to_slot):
        return pltpu.make_async_remote_copy(
            src_ref=modf_ref.at[to_slot],
            dst_ref=modf_ref.at[to_slot],
            send_sem=tsend_sem.at[d - 1],
            recv_sem=trecv_sem.at[to_slot],
            device_id={"tp": (t + d) % n_tp},
            device_id_type=MESH,
        )

    for d in range(1, n_tp):
        tp_copy(d, t).start()

    for d in hops[2:]:
        forward(d)

    for d in range(1, n_x):
        other = ((x + d) % n_x) * 2 + (1 - c)
        lat_copy(other, other, 0).wait_recv()
    lat_copy(partner, partner, 0).wait_recv()

    for b in range(n_tp):
        xv = x_ref[b].astype(F32)
        r = lax.rsqrt(jnp.mean(xv * xv, axis=-1, keepdims=True) + norm_eps)
        r_ref[pl.ds(b * rows, rows), :] = jnp.broadcast_to(r, (rows, LANES))

    neg_a = -decay_ref[0, 0]
    neg_b = -decay_ref[1, 0]
    cgain = cgain_ref[0]

    l_tab.wait()
    n_rows_total = tab_ref.shape[0] // 2 - GRID_W
    half = tab_ref.shape[1] // 2
    left = lax.broadcasted_iota(jnp.int32, (GRID_W, tab_ref.shape[1]), 1) < half

    def table(base):
        pieces = []
        for b in range(span // GRID_W):
            row = tab_ref[pl.ds(base + s * (span // GRID_W) + b, 1), :]
            col = tab_ref[pl.ds(base + n_rows_total, GRID_W), :]
            pieces.append(jnp.where(left, jnp.broadcast_to(row, col.shape), col))
        return jnp.concatenate(pieces, axis=0)

    cos_t = table(0)
    sin_t = table(n_rows_total + GRID_W)

    def rotate(v):
        u, w = v[:, : dk // 2], v[:, dk // 2 :]
        return jnp.concatenate([u * cos_t - w * sin_t, w * cos_t + u * sin_t], axis=1)

    l_gain.wait()
    l_wk.wait()
    l_wv.wait()
    for d in range(1, n_tp):
        tp_copy(n_tp - d, (t + d) % n_tp).wait_recv()

    cols_per = D // n_tp
    for k in range(D // LANES):
        cols = pl.ds(k * LANES, LANES)
        owner, off = divmod(k * LANES, cols_per)
        m = modf_ref[owner, :, pl.ds(off, LANES)]
        g = gain_ref[:, cols].astype(F32)
        f_lat = g * (1.0 + m[2:3])
        f_ctx = g * (1.0 + m[3:4])
        xv = x_ref[:, :, cols].reshape(span, LANES).astype(F32)
        h_ref[pl.ds(0, span), cols] = (xv * r_ref[pl.ds(0, span), :] * f_lat + m[0:1]).astype(BF16)
        cv = c_ref[:, cols].astype(F32)
        h_ref[pl.ds(span, ctx_rows), cols] = (cv * r_ref[pl.ds(span, ctx_rows), :] * f_ctx + m[1:2]).astype(BF16)

    kk = dot(h_ref[...], wk_ref[...]) * dk ** (-0.5)
    keys = rotate(kk[:span])
    k_ref[...] = keys.astype(BF16)
    keys = k_ref[...].astype(F32)
    ctx_key = kk[span:].astype(BF16).astype(F32)
    vv = dot(h_ref[...], wv_ref[...]).astype(BF16)
    v_ref[...] = vv[:span]
    values = vv[:span]
    ctx_val = vv[span:]

    place = lax.broadcasted_iota(jnp.int32, (span, 1), 0).astype(F32)
    fwd_keys = (keys * jnp.exp(neg_a * (span - 1.0 - place))).astype(BF16)
    bwd_keys = (keys * jnp.exp(neg_b * place)).astype(BF16)
    cplace = (lax.broadcasted_iota(jnp.int32, (ctx_rows, 1), 0) + s * ctx_rows).astype(F32)
    ctx_total = ctx_rows * n_sp
    cf_keys = (ctx_key * jnp.exp(neg_a * (ctx_total - 1.0 - cplace))).astype(BF16)
    cb_keys = (ctx_key * jnp.exp(neg_b * cplace)).astype(BF16)

    def scalar_exp(v):
        return jnp.exp(jnp.full((1, LANES), v, F32))[:, 0:1]

    sf = s.astype(F32)
    cf = cgain * dot_tokens(cf_keys, ctx_val)
    cf_ref[...] = cf
    lf_ref[...] = dot_tokens(fwd_keys, values) + scalar_exp(neg_a * (span * (sf + 1.0))) * cf
    cb = cgain * dot_tokens(cb_keys, ctx_val)
    cb_ref[...] = cb
    lb_ref[...] = dot_tokens(bwd_keys, values) + scalar_exp(neg_b * (span * (n_sp - sf))) * cb

    a_step = scalar_exp(neg_a * float(span))
    b_step = scalar_exp(neg_b * float(span))

    @pl.when(s == 0)
    def _():
        pr_ref[...] = jnp.zeros_like(pr_ref)

    @pl.when(s == n_sp - 1)
    def _():
        mr_ref[...] = jnp.zeros_like(mr_ref)

    def up_copy(j):
        return pltpu.make_async_remote_copy(
            src_ref=ps_ref.at[j],
            dst_ref=pr_ref.at[j],
            send_sem=pssem.at[j],
            recv_sem=prsem.at[j],
            device_id={"sp": (s + 1) % n_sp},
            device_id_type=MESH,
        )

    def down_copy(j):
        return pltpu.make_async_remote_copy(
            src_ref=ms_ref.at[j],
            dst_ref=mr_ref.at[j],
            send_sem=mssem.at[j],
            recv_sem=mrsem.at[j],
            device_id={"sp": (s + n_sp - 1) % n_sp},
            device_id_type=MESH,
        )

    def local_part():
        l_wq.wait()
        h = h_ref[pl.ds(0, span), :]
        query = rotate(dot(h, wq_ref[...])).astype(BF16)
        q_ref[...] = query
        scores = lax.dot_general(query, k_ref[...], (((1,), (1,)), ((), ())), preferred_element_type=F32)
        gap = (
            lax.broadcasted_iota(jnp.int32, (span, span), 0) - lax.broadcasted_iota(jnp.int32, (span, span), 1)
        ).astype(F32)
        mask = jnp.where(gap >= 0, jnp.exp(neg_a * jnp.maximum(gap, 0.0)), 0.0) + jnp.where(
            gap <= 0, jnp.exp(neg_b * jnp.maximum(-gap, 0.0)), 0.0
        )
        ret_ref[...] = dot((scores * mask).astype(BF16), v_ref[...])
        l_wg.wait()
        gp_ref[...] = silu(dot(h, wg_ref[...]))

    gap_s = n_sp - 1 - 2 * s
    early = s < n_sp // 2
    lag = jnp.minimum(jnp.where(early, gap_s, -gap_s) * LEAD, n_chunks)
    lag_up = jnp.where(early, 0, lag)
    lag_down = jnp.where(early, lag, 0)
    near_end = jnp.minimum(s, n_sp - 1 - s) < 4
    when_local = jnp.where(near_end, n_chunks, 0)

    def step(i, carry):
        @pl.when(i == when_local)
        def _():
            local_part()

        j_up = i - lag_up

        @pl.when((j_up >= 0) & (j_up < n_chunks))
        def _():
            j = j_up

            @pl.when(s > 0)
            def _():
                up_copy(j).wait_recv()

            @pl.when(s < n_sp - 1)
            def _():
                sl = pl.ds(pl.multiple_of(j * CHUNK, CHUNK), CHUNK)
                ps_ref[j, 0] = (a_step * pr_ref[j, 0].astype(F32) + lf_ref[sl, :]).astype(BF16)
                ps_ref[j, 1] = (pr_ref[j, 1].astype(F32) + cb_ref[sl, :]).astype(BF16)
                up_copy(j).start()

        j_dn = i - lag_down

        @pl.when((j_dn >= 0) & (j_dn < n_chunks))
        def _():
            j = j_dn

            @pl.when(s < n_sp - 1)
            def _():
                down_copy(j).wait_recv()

            @pl.when(s > 0)
            def _():
                sl = pl.ds(pl.multiple_of(j * CHUNK, CHUNK), CHUNK)
                ms_ref[j, 0] = (b_step * mr_ref[j, 0].astype(F32) + lb_ref[sl, :]).astype(BF16)
                ms_ref[j, 1] = (mr_ref[j, 1].astype(F32) + cf_ref[sl, :]).astype(BF16)
                down_copy(j).start()

        return carry

    lax.fori_loop(0, 2 * n_chunks, step, 0)

    ca = scalar_exp(neg_a * (span * sf))
    cbk = scalar_exp(neg_b * (span * (n_sp - 1.0 - sf)))
    up_in = pr_ref[...]
    down_in = mr_ref[...]
    s_fwd = up_in[:, 0].reshape(dk, dv).astype(F32) + ca * (
        down_in[:, 1].reshape(dk, dv).astype(F32) + cf_ref[...]
    )
    s_bwd = down_in[:, 0].reshape(dk, dv).astype(F32) + cbk * (
        up_in[:, 1].reshape(dk, dv).astype(F32) + cb_ref[...]
    )
    query = q_ref[...]
    ret = (
        ret_ref[...]
        + dot(query, s_fwd.astype(BF16)) * jnp.exp(neg_a * (place + 1.0))
        + dot(query, s_bwd.astype(BF16)) * jnp.exp(neg_b * (span - place))
    )
    centre = jnp.mean(ret, axis=-1, keepdims=True)
    ret = ret - centre
    variance = jnp.mean(ret * ret, axis=-1, keepdims=True)
    gated = (gp_ref[...] * (ret * lax.rsqrt(variance + norm_eps))).astype(BF16)
    g_ref[...] = gated.reshape(n_tp, rows, dv)

    l_wo.wait()

    def rows_of(core):
        return jnp.concatenate([g_ref[2 * k + core] for k in range(n_x)], axis=0)

    def pair_copy():
        return pltpu.make_async_remote_copy(
            src_ref=osend_ref,
            dst_ref=orecv_ref,
            send_sem=osend_sem,
            recv_sem=orecv_sem,
            device_id={"tp": partner},
            device_id_type=MESH,
        )

    osend_ref[...] = dot(rows_of(1 - c), wo_ref[...]).astype(BF16).reshape(n_x, rows, D)
    pair_copy().start()
    own_ref[...] = dot(rows_of(c), wo_ref[...]).reshape(n_x, rows, D)
    pair_copy().wait_recv()

    def out_copy(d):
        return pltpu.make_async_remote_copy(
            src_ref=xsend_ref.at[d - 1],
            dst_ref=xrecv_ref.at[d - 1],
            send_sem=rsend_sem.at[d - 1],
            recv_sem=rrecv_sem.at[d - 1],
            device_id={"tp": ((x + d) % n_x) * 2 + c},
            device_id_type=MESH,
        )

    for d in hops:
        to = (x + d) % n_x
        xsend_ref[d - 1] = (own_ref[to] + orecv_ref[to].astype(F32)).astype(BF16)
        out_copy(d).start()
    acc = own_ref[x] + orecv_ref[x].astype(F32)

    gtotal = gpart_ref[...]
    for d in range(1, n_sp):
        spg_copy(d).wait_recv()
        gtotal = gtotal + grecv_ref[d - 1]
    gatef_ref[t] = gtotal

    def tpg_copy(d, slot):
        return pltpu.make_async_remote_copy(
            src_ref=gatef_ref.at[slot],
            dst_ref=gatef_ref.at[slot],
            send_sem=hsend_sem.at[d - 1],
            recv_sem=hrecv_sem.at[slot],
            device_id={"tp": (t + d) % n_tp},
            device_id_type=MESH,
        )

    for d in range(1, n_tp):
        tpg_copy(d, t).start()
    for d in range(1, n_tp):
        tpg_copy(n_tp - d, (t + d) % n_tp).wait_recv()
    gate = jnp.concatenate([gatef_ref[k] for k in range(n_tp)], axis=1)

    for d in hops:
        out_copy(d).wait_recv()
        acc = acc + xrecv_ref[d - 1].astype(F32)
    out_ref[...] = (x_ref[t].astype(F32) + gate * acc).astype(BF16)

    for d in range(1, n_sp):
        sp_copy(d).wait_send()
        spg_copy(d).wait_send()
    for d in range(1, n_tp):
        tp_copy(d, t).wait_send()
        tpg_copy(d, t).wait_send()
    lat_copy(t, partner, 0).wait_send()
    for d in range(1, n_x):
        lat_copy(t, partner, d).wait_send()
        lat_copy(t, partner, n_x + d).wait_send()
        out_copy(d).wait_send()
    pair_copy().wait_send()

    @pl.when(s < n_sp - 1)
    def _():
        @pl.loop(0, n_chunks)
        def _(j):
            up_copy(j).wait_send()

    @pl.when(s > 0)
    def _():
        @pl.loop(0, n_chunks)
        def _(j):
            down_copy(j).wait_send()


def body(
    n_sp,
    n_tp,
    latent,
    cond,
    context,
    context_cond,
    norm_gain,
    mod_shift,
    mod_scale,
    mod_gate,
    w_query,
    w_key,
    w_value,
    w_gate,
    w_out,
    decay_rate,
    context_gain,
):
    rows, D = latent.shape
    span = rows * n_tp
    ctx_rows = context.shape[0]
    dk, dv = w_key.shape[1], w_value.shape[1]
    cols = D // n_tp
    n_x = n_tp // 2
    n_chunks = dk // CHUNK
    tab = jnp.asarray(rope_tables(span * n_sp // GRID_W, dk // 4))
    any_spec = pl.BlockSpec(memory_space=pl.ANY)
    smem = pl.BlockSpec(memory_space=pltpu.SMEM)
    dma = pltpu.SemaphoreType.DMA
    vm = pltpu.VMEM
    scratch = [
        vm((n_tp, rows, D), BF16),
        vm((ctx_rows, D), BF16),
        vm((2, cond.shape[0]), BF16),
        vm((1, D), BF16),
        vm(mod_shift.shape, BF16),
        vm(mod_scale.shape, BF16),
        vm(mod_gate.shape, BF16),
        vm(w_query.shape, BF16),
        vm(w_key.shape, BF16),
        vm(w_value.shape, BF16),
        vm(w_gate.shape, BF16),
        vm(w_out.shape, BF16),
        vm(tab.shape, F32),
        vm((4, cols), F32),
        vm((1, cols), F32),
        vm((n_sp - 1, 4, cols), F32),
        vm((n_sp - 1, 1, cols), F32),
        vm((n_tp, 4, cols), F32),
        vm((n_tp, 1, cols), F32),
        vm((span + ctx_rows, LANES), F32),
        vm((span + ctx_rows, D), BF16),
        vm((span, dk), BF16),
        vm((span, dv), BF16),
        vm((dk, dv), F32),
        vm((dk, dv), F32),
        vm((dk, dv), F32),
        vm((dk, dv), F32),
        vm((n_chunks, 2, CHUNK, dv), BF16),
        vm((n_chunks, 2, CHUNK, dv), BF16),
        vm((n_chunks, 2, CHUNK, dv), BF16),
        vm((n_chunks, 2, CHUNK, dv), BF16),
        vm((span, dk), BF16),
        vm((span, dv), F32),
        vm((span, dv), F32),
        vm((n_tp, rows, dv), BF16),
        vm((n_x, rows, D), BF16),
        vm((n_x, rows, D), BF16),
        vm((n_x, rows, D), F32),
        vm((n_x - 1, rows, D), BF16),
        vm((n_x - 1, rows, D), BF16),
        dma((13,)),
        dma((n_sp - 1,)),
        dma((n_sp - 1,)),
        dma((n_sp - 1,)),
        dma((n_sp - 1,)),
        dma((n_tp - 1,)),
        dma((n_tp,)),
        dma((n_tp - 1,)),
        dma((n_tp,)),
        dma((2 * n_x,)),
        dma((n_tp,)),
        dma((n_chunks,)),
        dma((n_chunks,)),
        dma((n_chunks,)),
        dma((n_chunks,)),
        dma,
        dma,
        dma((n_x - 1,)),
        dma((n_x - 1,)),
    ]
    return pl.pallas_call(
        functools.partial(kernel, n_sp, n_tp),
        out_shape=jax.ShapeDtypeStruct(latent.shape, BF16),
        in_specs=[smem, smem] + [any_spec] * 13,
        out_specs=pl.BlockSpec(memory_space=pltpu.VMEM),
        scratch_shapes=scratch,
        compiler_params=pltpu.CompilerParams(
            collective_id=0, has_side_effects=True, vmem_limit_bytes=60 * 1024 * 1024
        ),
        name="layer",
    )(
        decay_rate,
        context_gain,
        latent,
        jnp.stack([cond, context_cond]),
        context,
        norm_gain.reshape(1, D),
        mod_shift,
        mod_scale,
        mod_gate,
        w_query,
        w_key,
        w_value,
        w_gate,
        w_out,
        tab,
    )


def solution(mesh):
    return jax.shard_map(
        functools.partial(body, mesh.shape["sp"], mesh.shape["tp"]),
        mesh=mesh,
        in_specs=(
            P(("grp", "sp", "tp"), None),
            P(("grp", "sp")),
            P(("grp", "sp"), None),
            P("sp"),
            P(),
            P("sp", "tp"),
            P("sp", "tp"),
            P("sp", "tp"),
            P(None, "tp"),
            P(None, "tp"),
            P(None, "tp"),
            P(None, "tp"),
            P("tp", None),
            P(None, "tp"),
            P("tp"),
        ),
        out_specs=P(("grp", "sp", "tp"), None),
        check_vma=False,
    )
```

time: 340 us -> 121 us (0.36)
  Pallas kernels: 0 us -> 114 us
  other arithmetic: 94.1 us -> 1.26 us
  waiting for transfers between devices: 74.9 us -> 0 us
  blocking collectives: 67.7 us -> 0 us
  starting transfers between devices: 28.7 us -> 0 us
  matrix products: 27.7 us -> 0 us
  loops' own time: 21.6 us -> 0 us
  between operations: 15.7 us -> 0.66 us
    pallas_call x0 -> x1, Pallas kernels: none -> 114 us  [body(): pl.pallas_call(functools.partial(kernel, n_sp, n_tp), out_shape=jax.Shape...]
    select_n x32 -> x0, other arithmetic: 61.2 us -> none  [lap(): return jax.tree.map(lambda a, b: jnp.where(reached, a, b), new, before)]
    all_gather x3 -> x0, waiting for transfers between devices: 51.7 us -> none  [the longest x2 51.7 us: prefix(): lax.all_gather(part.astype(kind), axis)]
    all_to_all x2 -> x0, starting transfers between devices: 28.7 us -> none  [copy_for_each(): return lax.all_to_all(copies, axis, split_axis=0, concat_axis=0, tiled=True)]
    all_to_all x1 -> x0, blocking collectives: 28.4 us -> none  [sent_and_summed(): blocks = lax.all_to_all(in_blocks(x, dim, count), axis, 0, 0, tiled=True)]
    dot_general x21 -> x0, matrix products: 27.7 us -> none  [the longest x4 5.24 us: body(): jnp.dot(piece, weight, preferred_element_type=jnp.float32)]
    unnamed x1 -> x0, blocking collectives: 23.5 us -> none
    all_to_all x2 -> x0, waiting for transfers between devices: 22.4 us -> none  [copy_for_each(): return lax.all_to_all(copies, axis, split_axis=0, concat_axis=0, tiled=True)]
  transfers between devices with their start and end apart: 5 -> 0, of which waited for: 4 -> 0; matrix products, arithmetic and copies ran while one was open for 23% -> 0% of each run, Pallas kernels for 0% -> 0%
where the time goes in v1:
time: 121 us
  Pallas kernels  114 us (94%)
  local copies, waits for them, and re-layouts  4.16 us (3%)
  other arithmetic  1.26 us (1%)
    pallas_call x1, Pallas kernels, body(): pl.pallas_call(functools.partial(kernel, n_sp, n_tp), out_shape=jax.Shape...  114 us
    unnamed x2, local copies, waits for them, and re-layouts  2.87 us

profile of v1, /device:TPU:33, one launch (start us, length us, event | category | flops | bytes accessed | tf_op | source)
XLA Modules:
  0.0 120.5 jit_solution(7930722917308701439)
XLA Ops:
  0.7 1.3 %pad_maximum_fusion.cond_hbm = bf16[2,128]{1,0:T(2,128)(2,1)} fusion(bf16[1,128]{1,0:T(2,128)(2,1)} %bitcast.2, bf16[1,128]{1,0:T(2,128)(2,1)} %bitcast.3), kind=kLoop, calls=%fused_computation | loop fusion | flops 1024 | bytes 1024 | tf_op jit(solution)/shard_map/stack | solution.py:658
  1.9 1.3 %copy.17.decay_ref = f32[2,1]{1,0:T(2,128)} copy(f32[2,1]{0,1:T(1,128)} %param.29) | data formatting | bytes 16 | tf_op args[13]
  3.2 1.3 %reshape.3.gain_hbm = bf16[1,2048]{1,0:T(2,128)(2,1)} reshape(bf16[2048]{0:T(1024)(128)(2,1)} %param.20) | data formatting | bytes 8192 | tf_op jit(solution)/shard_map/reshape | solution.py:660
  4.5 114.4 %layer.1 = bf16[32,2048]{1,0:T(8,128)(2,1)} custom-call(f32[2,1]{1,0:T(2,128)} %copy.17.decay_ref, f32[1]{0:T(128)S(6)} %copy.19.cgain_ref, bf16[32,2048]{1,0:T(8,128)(2,1)} %latent_hbm.1, bf16[2,128]{1,0:T(2,128)(2,1)} %pad_maximum_fusion.cond_hbm, bf16[64,2048]{1,0:T(8,128)(2,1)} %context_hbm.1, bf16[1,2048]{1,0:T(2,128)(2,1)} %reshape.3.gain_hbm, ...), custom_call_target="tpu_custom_call" | custom-call | tf_op jit(solution)/shard_map/layer/pallas_call | solution.py:644
  119.0 1.6 %copy.20 = bf16[32,2048]{1,0:T(8,128)(2,1)} copy(bf16[32,2048]{1,0:T(8,128)(2,1)} %layer.1) | data formatting | bytes 262144

commit v2 on v1

--- a/solution.py
+++ b/solution.py
@@ -49,6 +49,7 @@
     cgain_ref,
     latent_hbm,
     cond_hbm,
+    ccond_hbm,
     context_hbm,
     gain_hbm,
     shift_hbm,
@@ -64,6 +65,7 @@
     x_ref,
     c_ref,
     cond_ref,
+    ccond_ref,
     gain_ref,
     mshift_ref,
     mscale_ref,
@@ -88,10 +90,15 @@
     lb_ref,
     cf_ref,
     cb_ref,
-    ps_ref,
-    pr_ref,
-    ms_ref,
-    mr_ref,
+    us_ref,
+    ur_ref,
+    ds_ref,
+    dr_ref,
+    bs_ref,
+    br_ref,
+    cs_ref,
+    cr_ref,
+    fin_ref,
     q_ref,
     gp_ref,
     ret_ref,
@@ -112,10 +119,14 @@
     hrecv_sem,
     xsend_sem,
     xrecv_sem,
-    pssem,
-    prsem,
-    mssem,
-    mrsem,
+    ussem,
+    ursem,
+    dssem,
+    drsem,
+    bssem,
+    brsem,
+    cssem,
+    crsem,
     osend_sem,
     orecv_sem,
     rsend_sem,
@@ -142,6 +153,7 @@
 
     l_lat = load(0, latent_hbm, x_ref.at[t])
     l_cond = load(1, cond_hbm, cond_ref)
+    l_ccond = load(13, ccond_hbm, ccond_ref)
     l_ms = load(2, shift_hbm, mshift_ref)
     l_mc = load(3, scale_hbm, mscale_ref)
     l_mg = load(4, gate_hbm, mgate_ref)
@@ -163,10 +175,10 @@
         pl.semaphore_signal(barrier, inc=1, device_id={"tp": (t + d) % n_tp}, device_id_type=MESH)
 
     l_cond.wait()
-    crows = silu(cond_ref[...].astype(F32))
-    rid = lax.broadcasted_iota(jnp.int32, (8, crows.shape[1]), 0)
-    cl = jnp.broadcast_to(crows[0:1], rid.shape)
-    cc = jnp.broadcast_to(crows[1:2], rid.shape)
+    l_ccond.wait()
+    rid = lax.broadcasted_iota(jnp.int32, (8, cond_ref.shape[1]), 0)
+    cl = jnp.broadcast_to(silu(cond_ref[...].astype(F32)), rid.shape)
+    cc = jnp.broadcast_to(silu(ccond_ref[...].astype(F32)), rid.shape)
     lhs_shift = jnp.where(rid == 0, cl, jnp.where(rid == 1, cc, 0.0)).astype(BF16)
     lhs_scale = jnp.where(rid == 2, cl, jnp.where(rid == 3, cc, 0.0)).astype(BF16)
     lhs_gate = jnp.where(rid == 0, cl, 0.0).astype(BF16)
@@ -268,8 +280,8 @@
         r = lax.rsqrt(jnp.mean(xv * xv, axis=-1, keepdims=True) + norm_eps)
         r_ref[pl.ds(b * rows, rows), :] = jnp.broadcast_to(r, (rows, LANES))
 
-    neg_a = -decay_ref[0, 0]
-    neg_b = -decay_ref[1, 0]
+    neg_a = -decay_ref[0]
+    neg_b = -decay_ref[1]
     cgain = cgain_ref[0]
 
     l_tab.wait()
@@ -303,7 +315,7 @@
         cols = pl.ds(k * LANES, LANES)
         owner, off = divmod(k * LANES, cols_per)
         m = modf_ref[owner, :, pl.ds(off, LANES)]
-        g = gain_ref[:, cols].astype(F32)
+        g = gain_ref[k : k + 1, :].astype(F32)
         f_lat = g * (1.0 + m[2:3])
         f_ctx = g * (1.0 + m[3:4])
         xv = x_ref[:, :, cols].reshape(span, LANES).astype(F32)
@@ -343,33 +355,58 @@
     a_step = scalar_exp(neg_a * float(span))
     b_step = scalar_exp(neg_b * float(span))
 
-    @pl.when(s == 0)
-    def _():
-        pr_ref[...] = jnp.zeros_like(pr_ref)
-
-    @pl.when(s == n_sp - 1)
-    def _():
-        mr_ref[...] = jnp.zeros_like(mr_ref)
-
-    def up_copy(j):
+    top, mid, low = n_sp - 1, n_sp // 2, n_sp // 4
+
+    def chain(send, recv, ssem, rsem, to):
+        def copy(j, src=None):
+            return pltpu.make_async_remote_copy(
+                src_ref=(send if src is None else src).at[j],
+                dst_ref=recv.at[j],
+                send_sem=ssem,
+                recv_sem=rsem.at[j],
+                device_id={"sp": to},
+                device_id_type=MESH,
+            )
+
+        return copy
+
+    above, under = (s + 1) % n_sp, (s + n_sp - 1) % n_sp
+    up_copy = chain(us_ref, ur_ref, ussem, ursem, above)
+    down_copy = chain(ds_ref, dr_ref, dssem, drsem, under)
+    below_copy = chain(bs_ref, br_ref, bssem, brsem, under)
+    carry_copy = chain(cs_ref, cr_ref, cssem, crsem, above)
+    up_recv, up_send = s > 0, s < top
+    down_recv, down_send = (s >= low) & (s < top), s > low
+    below_recv, below_send = s < mid - 1, (s > 0) & (s < mid)
+    carry_recv, carry_send = (s > mid) | (s < low), s >= mid
+    carry_pass = s < low - 1
+
+    for first, ref in ((0, ur_ref), (top, dr_ref), (mid - 1, br_ref), (mid, cr_ref)):
+
+        @pl.when(s == first)
+        def _(ref=ref):
+            ref[...] = jnp.zeros_like(ref)
+
+    carry_w = scalar_exp(neg_b * (span * jnp.maximum(sf - mid, 0.0)))
+
+    gtotal = gpart_ref[...]
+    for d in range(1, n_sp):
+        spg_copy(d).wait_recv()
+        gtotal = gtotal + grecv_ref[d - 1]
+    gatef_ref[t] = gtotal
+
+    def tpg_copy(d, slot):
         return pltpu.make_async_remote_copy(
-            src_ref=ps_ref.at[j],
-            dst_ref=pr_ref.at[j],
-            send_sem=pssem.at[j],
-            recv_sem=prsem.at[j],
-            device_id={"sp": (s + 1) % n_sp},
+            src_ref=gatef_ref.at[slot],
+            dst_ref=gatef_ref.at[slot],
+            send_sem=hsend_sem.at[d - 1],
+            recv_sem=hrecv_sem.at[slot],
+            device_id={"tp": (t + d) % n_tp},
             device_id_type=MESH,
         )
 
-    def down_copy(j):
-        return pltpu.make_async_remote_copy(
-            src_ref=ms_ref.at[j],
-            dst_ref=mr_ref.at[j],
-            send_sem=mssem.at[j],
-            recv_sem=mrsem.at[j],
-            device_id={"sp": (s + n_sp - 1) % n_sp},
-            device_id_type=MESH,
-        )
+    for d in range(1, n_tp):
+        tpg_copy(d, t).start()
 
     def local_part():
         l_wq.wait()
@@ -387,67 +424,121 @@
         l_wg.wait()
         gp_ref[...] = silu(dot(h, wg_ref[...]))
 
-    gap_s = n_sp - 1 - 2 * s
-    early = s < n_sp // 2
-    lag = jnp.minimum(jnp.where(early, gap_s, -gap_s) * LEAD, n_chunks)
-    lag_up = jnp.where(early, 0, lag)
-    lag_down = jnp.where(early, lag, 0)
-    near_end = jnp.minimum(s, n_sp - 1 - s) < 4
-    when_local = jnp.where(near_end, n_chunks, 0)
+    late = 4 * n_sp
+    at_up = s
+    at_down = jnp.where(s >= low, top - s, late)
+    at_below = jnp.where(s < mid, mid - 1 - s, late)
+    at_carry = jnp.where(s >= mid, s - mid, jnp.where(s < low, s + n_sp - mid, late))
+    first = jnp.minimum(jnp.minimum(at_up, at_down), jnp.minimum(at_below, at_carry))
+    lag_up = (at_up - first) * LEAD
+    lag_down = (at_down - first) * LEAD
+    lag_below = (at_below - first) * LEAD
+    lag_carry = (at_carry - first) * LEAD
+    n_steps = n_chunks + n_sp * LEAD
+
+    when_local = 0
+    for k in range(n_sp):
+        if k in (0, mid - 1, mid, top):
+            at = n_chunks
+        elif k in (mid - 2, mid + 1):
+            at = n_steps - 1
+        elif k == top - 1:
+            at = n_chunks + 5 * LEAD
+        else:
+            at = 0
+        when_local = when_local + jnp.where(s == k, at, 0)
+
+    def active(j):
+        return (j >= 0) & (j < n_chunks)
 
     def step(i, carry):
         @pl.when(i == when_local)
         def _():
             local_part()
 
+        def rows_at(j):
+            return pl.ds(pl.multiple_of(j * CHUNK, CHUNK), CHUNK)
+
         j_up = i - lag_up
 
-        @pl.when((j_up >= 0) & (j_up < n_chunks))
+        @pl.when(active(j_up))
         def _():
-            j = j_up
-
-            @pl.when(s > 0)
-            def _():
-                up_copy(j).wait_recv()
-
-            @pl.when(s < n_sp - 1)
-            def _():
-                sl = pl.ds(pl.multiple_of(j * CHUNK, CHUNK), CHUNK)
-                ps_ref[j, 0] = (a_step * pr_ref[j, 0].astype(F32) + lf_ref[sl, :]).astype(BF16)
-                ps_ref[j, 1] = (pr_ref[j, 1].astype(F32) + cb_ref[sl, :]).astype(BF16)
-                up_copy(j).start()
+            @pl.when(up_recv)
+            def _():
+                up_copy(j_up).wait_recv()
+
+            @pl.when(up_send)
+            def _():
+                us_ref[j_up, 0] = (a_step * ur_ref[j_up, 0].astype(F32) + lf_ref[rows_at(j_up), :]).astype(BF16)
+                us_ref[j_up, 1] = (ur_ref[j_up, 1].astype(F32) + cb_ref[rows_at(j_up), :]).astype(BF16)
+                up_copy(j_up).start()
+
+        j_ca = i - lag_carry
+
+        @pl.when(active(j_ca) & (carry_recv | carry_send))
+        def _():
+            @pl.when(carry_recv)
+            def _():
+                carry_copy(j_ca).wait_recv()
+
+            @pl.when(carry_pass)
+            def _():
+                carry_copy(j_ca, cr_ref).start()
+
+            @pl.when(carry_send)
+            def _():
+                cs_ref[j_ca, 0] = (cr_ref[j_ca, 0].astype(F32) + carry_w * lb_ref[rows_at(j_ca), :]).astype(BF16)
+                cs_ref[j_ca, 1] = (cr_ref[j_ca, 1].astype(F32) + cf_ref[rows_at(j_ca), :]).astype(BF16)
+                carry_copy(j_ca).start()
 
         j_dn = i - lag_down
 
-        @pl.when((j_dn >= 0) & (j_dn < n_chunks))
+        @pl.when(active(j_dn) & (down_recv | down_send))
         def _():
-            j = j_dn
-
-            @pl.when(s < n_sp - 1)
-            def _():
-                down_copy(j).wait_recv()
-
-            @pl.when(s > 0)
-            def _():
-                sl = pl.ds(pl.multiple_of(j * CHUNK, CHUNK), CHUNK)
-                ms_ref[j, 0] = (b_step * mr_ref[j, 0].astype(F32) + lb_ref[sl, :]).astype(BF16)
-                ms_ref[j, 1] = (mr_ref[j, 1].astype(F32) + cf_ref[sl, :]).astype(BF16)
-                down_copy(j).start()
+            @pl.when(down_recv)
+            def _():
+                down_copy(j_dn).wait_recv()
+
+            @pl.when(down_send)
+            def _():
+                ds_ref[j_dn, 0] = (b_step * dr_ref[j_dn, 0].astype(F32) + lb_ref[rows_at(j_dn), :]).astype(BF16)
+                ds_ref[j_dn, 1] = (dr_ref[j_dn, 1].astype(F32) + cf_ref[rows_at(j_dn), :]).astype(BF16)
+                down_copy(j_dn).start()
+
+        j_be = i - lag_below
+
+        @pl.when(active(j_be) & (below_recv | below_send))
+        def _():
+            @pl.when(below_recv)
+            def _():
+                below_copy(j_be).wait_recv()
+
+            @pl.when(below_send)
+            def _():
+                bs_ref[j_be, 0] = (b_step * br_ref[j_be, 0].astype(F32) + lb_ref[rows_at(j_be), :]).astype(BF16)
+                bs_ref[j_be, 1] = (br_ref[j_be, 1].astype(F32) + cf_ref[rows_at(j_be), :]).astype(BF16)
+                below_copy(j_be).start()
 
         return carry
 
-    lax.fori_loop(0, 2 * n_chunks, step, 0)
+    lax.fori_loop(0, n_steps, step, 0)
 
     ca = scalar_exp(neg_a * (span * sf))
     cbk = scalar_exp(neg_b * (span * (n_sp - 1.0 - sf)))
-    up_in = pr_ref[...]
-    down_in = mr_ref[...]
-    s_fwd = up_in[:, 0].reshape(dk, dv).astype(F32) + ca * (
-        down_in[:, 1].reshape(dk, dv).astype(F32) + cf_ref[...]
-    )
-    s_bwd = down_in[:, 0].reshape(dk, dv).astype(F32) + cbk * (
-        up_in[:, 1].reshape(dk, dv).astype(F32) + cb_ref[...]
-    )
+    low_w = scalar_exp(neg_b * (span * jnp.maximum(mid - 1.0 - sf, 0.0)))
+
+    @pl.when(s >= low)
+    def _():
+        fin_ref[0] = dr_ref[:, 0].reshape(dk, dv).astype(F32)
+        fin_ref[1] = dr_ref[:, 1].reshape(dk, dv).astype(F32)
+
+    @pl.when(s < low)
+    def _():
+        fin_ref[0] = br_ref[:, 0].reshape(dk, dv).astype(F32) + low_w * cr_ref[:, 0].reshape(dk, dv).astype(F32)
+        fin_ref[1] = br_ref[:, 1].reshape(dk, dv).astype(F32) + cr_ref[:, 1].reshape(dk, dv).astype(F32)
+
+    s_fwd = ur_ref[:, 0].reshape(dk, dv).astype(F32) + ca * (fin_ref[1] + cf_ref[...])
+    s_bwd = fin_ref[0] + cbk * (ur_ref[:, 1].reshape(dk, dv).astype(F32) + cb_ref[...])
     query = q_ref[...]
     ret = (
         ret_ref[...]
@@ -496,24 +587,6 @@
         out_copy(d).start()
     acc = own_ref[x] + orecv_ref[x].astype(F32)
 
-    gtotal = gpart_ref[...]
-    for d in range(1, n_sp):
-        spg_copy(d).wait_recv()
-        gtotal = gtotal + grecv_ref[d - 1]
-    gatef_ref[t] = gtotal
-
-    def tpg_copy(d, slot):
-        return pltpu.make_async_remote_copy(
-            src_ref=gatef_ref.at[slot],
-            dst_ref=gatef_ref.at[slot],
-            send_sem=hsend_sem.at[d - 1],
-            recv_sem=hrecv_sem.at[slot],
-            device_id={"tp": (t + d) % n_tp},
-            device_id_type=MESH,
-        )
-
-    for d in range(1, n_tp):
-        tpg_copy(d, t).start()
     for d in range(1, n_tp):
         tpg_copy(n_tp - d, (t + d) % n_tp).wait_recv()
     gate = jnp.concatenate([gatef_ref[k] for k in range(n_tp)], axis=1)
@@ -536,17 +609,15 @@
         out_copy(d).wait_send()
     pair_copy().wait_send()
 
-    @pl.when(s < n_sp - 1)
-    def _():
-        @pl.loop(0, n_chunks)
-        def _(j):
-            up_copy(j).wait_send()
-
-    @pl.when(s > 0)
-    def _():
-        @pl.loop(0, n_chunks)
-        def _(j):
-            down_copy(j).wait_send()
+    def all_sent(cond, send, sem):
+        @pl.when(cond)
+        def _():
+            pltpu.make_async_copy(send, send, sem).wait()
+
+    all_sent(up_send, us_ref, ussem)
+    all_sent(down_send, ds_ref, dssem)
+    all_sent(below_send, bs_ref, bssem)
+    all_sent(carry_send | carry_pass, cs_ref, cssem)
 
 
 def body(
@@ -583,8 +654,9 @@
     scratch = [
         vm((n_tp, rows, D), BF16),
         vm((ctx_rows, D), BF16),
-        vm((2, cond.shape[0]), BF16),
-        vm((1, D), BF16),
+        vm((1, cond.shape[0]), BF16),
+        vm((1, cond.shape[0]), BF16),
+        vm((D // LANES, LANES), BF16),
         vm(mod_shift.shape, BF16),
         vm(mod_scale.shape, BF16),
         vm(mod_gate.shape, BF16),
@@ -612,6 +684,11 @@
         vm((n_chunks, 2, CHUNK, dv), BF16),
         vm((n_chunks, 2, CHUNK, dv), BF16),
         vm((n_chunks, 2, CHUNK, dv), BF16),
+        vm((n_chunks, 2, CHUNK, dv), BF16),
+        vm((n_chunks, 2, CHUNK, dv), BF16),
+        vm((n_chunks, 2, CHUNK, dv), BF16),
+        vm((n_chunks, 2, CHUNK, dv), BF16),
+        vm((2, dk, dv), F32),
         vm((span, dk), BF16),
         vm((span, dv), F32),
         vm((span, dv), F32),
@@ -621,7 +698,7 @@
         vm((n_x, rows, D), F32),
         vm((n_x - 1, rows, D), BF16),
         vm((n_x - 1, rows, D), BF16),
-        dma((13,)),
+        dma((14,)),
         dma((n_sp - 1,)),
         dma((n_sp - 1,)),
         dma((n_sp - 1,)),
@@ -632,9 +709,13 @@
         dma((n_tp,)),
         dma((2 * n_x,)),
         dma((n_tp,)),
+        dma,
         dma((n_chunks,)),
+        dma,
         dma((n_chunks,)),
+        dma,
         dma((n_chunks,)),
+        dma,
         dma((n_chunks,)),
         dma,
         dma,
@@ -644,7 +725,7 @@
     return pl.pallas_call(
         functools.partial(kernel, n_sp, n_tp),
         out_shape=jax.ShapeDtypeStruct(latent.shape, BF16),
-        in_specs=[smem, smem] + [any_spec] * 13,
+        in_specs=[smem, smem] + [any_spec] * 14,
         out_specs=pl.BlockSpec(memory_space=pltpu.VMEM),
         scratch_shapes=scratch,
         compiler_params=pltpu.CompilerParams(
@@ -652,12 +733,13 @@
         ),
         name="layer",
     )(
-        decay_rate,
+        decay_rate.reshape(2),
         context_gain,
         latent,
-        jnp.stack([cond, context_cond]),
+        cond.reshape(1, -1),
+        context_cond.reshape(1, -1),
         context,
-        norm_gain.reshape(1, D),
+        norm_gain.reshape(D // LANES, LANES),
         mod_shift,
         mod_scale,
         mod_gate,

time: 121 us -> 98.2 us (0.81)
  the two profiles are of different devices: /device:TPU:33 before, /device:TPU:417 now
where the time goes in v2:
time: 98.2 us; the launch traced here: 98 us
  Pallas kernels  95.8 us (98%)
  local copies, waits for them, and re-layouts  1.57 us (2%)
    pallas_call x1, Pallas kernels, body(): pl.pallas_call(functools.partial(kernel, n_sp, n_tp), out_shape=jax.Shape...  95.8 us

profile of v2, /device:TPU:417, one launch (start us, length us, event | category | flops | bytes accessed | tf_op | source)
XLA Modules:
  0.0 98.0 jit_solution(16946296964258831805)
XLA Ops:
  0.7 95.8 %layer.1 = bf16[32,2048]{1,0:T(8,128)(2,1)} custom-call(f32[2]{0:T(128)} %bitcast.5, f32[1]{0:T(128)S(6)} %copy.18.cgain_ref, bf16[32,2048]{1,0:T(8,128)(2,1)} %latent_hbm.1, bf16[1,128]{1,0:T(2,128)(2,1)} %bitcast.6, bf16[1,128]{1,0:T(2,128)(2,1)} %bitcast.7, bf16[64,2048]{1,0:T(8,128)(2,1)} %context_hbm.1, bf16[16,128]{1,0:T(8,128)(2,1)} %bitcast.4, ...), custom_call_target="tpu_custom_call" | custom-call | tf_op jit(solution)/shard_map/layer/pallas_call | solution.py:725
  96.5 1.6 %copy.19 = bf16[32,2048]{1,0:T(8,128)(2,1)} copy(bf16[32,2048]{1,0:T(8,128)(2,1)} %layer.1) | data formatting | bytes 262144
